TPU v7x, 256 devices: a 4x2x16 block of a 4x16x16 slice. The times are simulated.
256 devices in a mesh: grp: 2 (over y), sp: 32 (over z, core), tp: 4 (over x).
Axes of the slice: x: 4, y: 2, z: 16, core: 2. Of those that a mesh axis runs over, the one named last changes fastest.
The devices are a block of a 4x16x16 slice.
Arguments:
- latent: bfloat16 [16384, 512], P(('grp', 'sp')), parts along dimension 0, may hold values from -6 to 6
- rope_key: bfloat16 [16384, 64], P(('grp', 'sp')), parts along dimension 0, may hold values from -6 to 6
- wide_query: bfloat16 [16384, 1536], P(('grp', 'sp'), 'tp'), parts along dimension 0, may hold values from -1300 to 1300
- narrow_query: bfloat16 [16384, 1024], P(('grp', 'sp'), 'tp'), parts along dimension 0, may hold values from -1300 to 1300
- wide_key_weight: bfloat16 [512, 1024], P(None, 'tp'), may hold values from -0.25 to 0.25
- wide_value_weight: bfloat16 [512, 1024], P(None, 'tp'), may hold values from -0.25 to 0.25
- narrow_key_weight: bfloat16 [512, 512], P(None, 'tp'), may hold values from -0.25 to 0.25
- narrow_value_weight: bfloat16 [512, 512], P(None, 'tp'), may hold values from -0.25 to 0.25
- latent_norm_scale: float32 [512], replicated, may hold values from 0.1 to 1.9
- out_wide: bfloat16 [1024, 4096], P('tp'), may hold values from -0.4375 to 0.4375
- out_narrow: bfloat16 [512, 4096], P('tp'), may hold values from -0.4375 to 0.4375
- residual: bfloat16 [16384, 4096], P(('grp', 'sp', 'tp')), parts along dimension 0, may hold values from -6 to 6
- ffn_gain: float32 [4096], replicated, may hold values from 0.1 to 1.9
- shared_gate: bfloat16 [4096, 512], P(None, 'tp'), may hold values from -0.09375 to 0.09375
- shared_up: bfloat16 [4096, 512], P(None, 'tp'), may hold values from -0.09375 to 0.09375
- shared_down: bfloat16 [512, 4096], P('tp'), may hold values from -0.25 to 0.25
- expert_gate: bfloat16 [128, 4096, 192], P(('sp', 'tp')), may hold values from -0.09375 to 0.09375
- expert_up: bfloat16 [128, 4096, 192], P(('sp', 'tp')), may hold values from -0.09375 to 0.09375
- expert_down: bfloat16 [128, 192, 4096], P(('sp', 'tp')), may hold values from -0.4375 to 0.4375
- routes: int32 [16384, 2], P(('grp', 'sp', 'tp')), parts along dimension 0, may hold values from 0 to 127, all different within a row; in each aligned block of 64 rows (0 to 63, 64 to 127, ...) at most 2 rows name the same one
- route_weights: float32 [16384, 2], P(('grp', 'sp', 'tp')), parts along dimension 0, may hold values from 0.25 to 1.5
Outputs:
- layer_out: bfloat16 [16384, 4096], P(('grp', 'sp', 'tp')), parts along dimension 0
There are 2 independent parts, one for each index of `grp`. A program takes and returns all parts, laid end to end along the dimension named above; an argument that names none is the same for every part. Nothing has to cross between parts.
Inputs may be any that keep to these rules, and one draw needn't show every extreme that they name: `routes`: each row names 2 different experts; in each aligned block of 64 rows no expert is named by more than 2 rows, and some block has an expert named exactly 2 times.
All inputs are finite; a program needn't handle non-finite values.
Results may differ from a plain program's by a relative error of at most 0.023.
Values may be sent and summed in bfloat16 or wider, within the bound.
A program may use at most 128 MiB of HBM per device.

v0:
```python
import math
import jax
import jax.numpy as jnp
from jax import lax
from jax.sharding import PartitionSpec as P

ROPE = 64
WIDE_HEAD_SIZE = 128
NARROW_HEAD_SIZE = 64
EPS = 1e-06
ROPE_BASE = 10000.0
NEG_FILL = -1e30


def sent_together(arrays, axis, dim, along):
    both = jnp.concatenate(arrays, axis=along)
    whole, at, outs = (lax.all_gather(both, axis, axis=dim, tiled=True), 0, [])
    for a in arrays:
        outs.append(lax.slice_in_dim(whole, at, at + a.shape[along], axis=along))
        at += a.shape[along]
    return tuple(outs)


def split_up(array, dim, peers):
    before, after = (array.shape[:dim], array.shape[dim + 1 :])
    return jnp.moveaxis(array.reshape(*before, peers, -1, *after), dim, 0)


def summed_on_arrival(array, axis, dim):
    peers = lax.axis_size(axis)
    blocks = lax.all_to_all(split_up(array, dim, peers), axis, 0, 0, tiled=True)
    return jnp.sum(blocks.astype(jnp.float32), axis=0)


def rotate(values, positions):
    half_size = values.shape[-1] // 2
    inverse = ROPE_BASE ** (-jnp.arange(half_size, dtype=jnp.float32) * 2.0 / values.shape[-1])
    angles = positions.astype(jnp.float32)[:, None] * inverse[None, :]
    shaped = (angles.shape[0],) + (1,) * (values.ndim - 2) + (half_size,)
    cosine_table = jnp.cos(angles).reshape(shaped)
    sine_table = jnp.sin(angles).reshape(shaped)
    first_half = values[..., :half_size]
    second_half = values[..., half_size:]
    return jnp.concatenate(
        [
            first_half * cosine_table - second_half * sine_table,
            second_half * cosine_table + first_half * sine_table,
        ],
        axis=-1,
    )


def rms_scale(values, gain):
    return values * lax.rsqrt(jnp.mean(values * values, axis=-1, keepdims=True) + EPS) * gain


def update(state, query_plain, query_turned, keys, turned_rows, values, visible, factor):
    running_max, running_sum, weighted = state
    scores = jnp.einsum("qhd,khd->hqk", query_plain, keys, preferred_element_type=jnp.float32)
    scores = scores + jnp.einsum(
        "qhr,kr->hqk", query_turned, turned_rows, preferred_element_type=jnp.float32
    )
    scores = jnp.where(visible[None], scores * factor, NEG_FILL)
    new_max = jnp.maximum(running_max, jnp.max(scores, axis=2))
    probs = jnp.where(visible[None], jnp.exp(scores - new_max[:, :, None]), 0.0)
    fading = jnp.exp(running_max - new_max)
    running_sum = running_sum * fading + jnp.sum(probs, axis=2)
    weighted = weighted * fading[:, :, None] + jnp.einsum(
        "hqk,khd->hqd", probs.astype(jnp.bfloat16), values, preferred_element_type=jnp.float32
    )
    return (new_max, running_sum, weighted)


def empty_state(heads, queries, value_size):
    return (
        jnp.full((heads, queries), NEG_FILL, jnp.float32),
        jnp.zeros((heads, queries), jnp.float32),
        jnp.zeros((heads, queries, value_size), jnp.float32),
    )


def finish(state):
    normal_sampler = state[2] / state[1][:, :, None]
    heads, queries, value_size = normal_sampler.shape
    return (
        normal_sampler.astype(jnp.bfloat16).transpose(1, 0, 2).reshape(queries, heads * value_size)
    )


def body(
    latent,
    rope_key,
    wide_query,
    narrow_query,
    wide_key_weight,
    wide_value_weight,
    narrow_key_weight,
    narrow_value_weight,
    latent_norm_scale,
    out_wide,
    out_narrow,
    residual,
    ffn_gain,
    shared_gate,
    shared_up,
    shared_down,
    expert_gate,
    expert_up,
    expert_down,
    routes,
    route_weights,
):
    tok_dev = latent.shape[0]
    seq_index = lax.axis_index("sp")
    own_pos = seq_index * tok_dev + jnp.arange(tok_dev, dtype=jnp.int32)
    last_pos = seq_index * tok_dev + tok_dev - 1
    normed_latent = rms_scale(latent.astype(jnp.float32), latent_norm_scale).astype(jnp.bfloat16)
    turned_key = rotate(rope_key.astype(jnp.float32), own_pos).astype(jnp.bfloat16)
    wide_heads_q = wide_query.reshape(tok_dev, -1, WIDE_HEAD_SIZE + ROPE)
    wide_plain = wide_heads_q[..., :WIDE_HEAD_SIZE]
    wide_turned = rotate(wide_heads_q[..., WIDE_HEAD_SIZE:].astype(jnp.float32), own_pos).astype(
        jnp.bfloat16
    )
    narrow_heads_q = narrow_query.reshape(tok_dev, -1, NARROW_HEAD_SIZE + ROPE)
    narrow_plain = narrow_heads_q[..., :NARROW_HEAD_SIZE]
    narrow_turned = rotate(
        narrow_heads_q[..., NARROW_HEAD_SIZE:].astype(jnp.float32), own_pos
    ).astype(jnp.bfloat16)
    wide_local = wide_plain.shape[1]
    narrow_local = narrow_plain.shape[1]
    wide_factor = (WIDE_HEAD_SIZE + ROPE) ** (-0.5)
    narrow_factor = (NARROW_HEAD_SIZE + ROPE) ** (-0.5)
    initial = empty_state(wide_local, tok_dev, WIDE_HEAD_SIZE) + empty_state(
        narrow_local, tok_dev, NARROW_HEAD_SIZE
    )
    pieces = sent_together((normed_latent, turned_key), "sp", 0, 1)
    indices = jnp.arange(pieces[0].shape[0], dtype=jnp.int32)
    placing = lambda positions: positions
    latent_rows, turned_rows = pieces
    length_rows = latent_rows.shape[0]
    block = math.gcd(length_rows, 512)

    def one_block(block_index, inner):
        lat_block = lax.dynamic_slice_in_dim(latent_rows, block_index * block, block, 0)
        turned_block = lax.dynamic_slice_in_dim(turned_rows, block_index * block, block, 0)
        key_pos = placing(lax.dynamic_slice_in_dim(indices, block_index * block, block, 0))

        def work(current):
            visible = key_pos[None, :] <= own_pos[:, None]
            wide_keys = (
                jnp.dot(lat_block, wide_key_weight, preferred_element_type=jnp.float32)
                .astype(jnp.bfloat16)
                .reshape(block, wide_local, WIDE_HEAD_SIZE)
            )
            wide_values = (
                jnp.dot(lat_block, wide_value_weight, preferred_element_type=jnp.float32)
                .astype(jnp.bfloat16)
                .reshape(block, wide_local, WIDE_HEAD_SIZE)
            )
            narrow_keys = (
                jnp.dot(lat_block, narrow_key_weight, preferred_element_type=jnp.float32)
                .astype(jnp.bfloat16)
                .reshape(block, narrow_local, NARROW_HEAD_SIZE)
            )
            narrow_values = (
                jnp.dot(lat_block, narrow_value_weight, preferred_element_type=jnp.float32)
                .astype(jnp.bfloat16)
                .reshape(block, narrow_local, NARROW_HEAD_SIZE)
            )
            wide_state = update(
                current[:3],
                wide_plain,
                wide_turned,
                wide_keys,
                turned_block,
                wide_values,
                visible,
                wide_factor,
            )
            narrow_state = update(
                current[3:],
                narrow_plain,
                narrow_turned,
                narrow_keys,
                turned_block,
                narrow_values,
                visible,
                narrow_factor,
            )
            return wide_state + narrow_state

        return lax.cond(jnp.min(key_pos) <= last_pos, work, lambda current: current, inner)

    final = lax.fori_loop(0, length_rows // block, one_block, initial)
    wide_mix = finish(final[:3])
    narrow_mix = finish(final[3:])
    projected = summed_on_arrival(
        (
            jnp.dot(wide_mix, out_wide, preferred_element_type=jnp.float32)
            + jnp.dot(narrow_mix, out_narrow, preferred_element_type=jnp.float32)
        ).astype(jnp.bfloat16),
        "tp",
        0,
    )
    stream = (residual.astype(jnp.float32) + projected).astype(jnp.bfloat16)
    normed = rms_scale(stream.astype(jnp.float32), ffn_gain).astype(jnp.bfloat16)
    piece = lax.all_gather(normed, "tp", axis=0, tiled=True)
    gate_part = jnp.dot(piece, shared_gate, preferred_element_type=jnp.float32)
    up_part = jnp.dot(piece, shared_up, preferred_element_type=jnp.float32)
    active = (jax.nn.silu(gate_part) * up_part).astype(jnp.bfloat16)
    shared_terms = jnp.dot(active, shared_down, preferred_element_type=jnp.float32)
    shared = lax.psum_scatter(
        shared_terms.astype(jnp.bfloat16), "tp", scatter_dimension=0, tiled=True
    ).astype(jnp.float32)
    rows_here, top_count = routes.shape
    local_experts = expert_gate.shape[0]
    experts_all = local_experts * lax.axis_size(("sp", "tp"))
    capacity = max(2, 2 * top_count * rows_here // experts_all)
    model_width = normed.shape[1]
    flat_routes = routes.reshape(-1)
    assigned = flat_routes.shape[0]
    choose = (flat_routes[:, None] == jnp.arange(experts_all, dtype=jnp.int32)[None, :]).astype(
        jnp.float32
    )
    lower_mask = (jnp.arange(assigned)[:, None] > jnp.arange(assigned)[None, :]).astype(jnp.float32)
    earlier = jnp.dot(lower_mask, choose, precision=lax.Precision.HIGHEST)
    slots = jnp.sum(earlier * choose, axis=1).astype(jnp.int32)
    target = flat_routes * capacity + slots
    send_map = jnp.any(
        target.reshape(rows_here, top_count)[None, :, :]
        == jnp.arange(experts_all * capacity, dtype=jnp.int32)[:, None, None],
        axis=2,
    ).astype(jnp.bfloat16)
    outgoing = jnp.dot(send_map, normed, preferred_element_type=jnp.float32).astype(jnp.bfloat16)
    outgoing = outgoing.reshape(experts_all, capacity, model_width)
    incoming = lax.all_to_all(outgoing, ("sp", "tp"), split_axis=0, concat_axis=0, tiled=True)
    sources = incoming.shape[0] // local_experts
    grouped = incoming.reshape(sources, local_experts, incoming.shape[1], model_width)
    gate_part = jnp.einsum(
        "sxcd,xdf->sxcf", grouped, expert_gate, preferred_element_type=jnp.float32
    )
    up_part = jnp.einsum("sxcd,xdf->sxcf", grouped, expert_up, preferred_element_type=jnp.float32)
    active = (jax.nn.silu(gate_part) * up_part).astype(jnp.bfloat16)
    finished = jnp.einsum(
        "sxcf,xfd->sxcd", active, expert_down, preferred_element_type=jnp.float32
    ).astype(jnp.bfloat16)
    returned = lax.all_to_all(
        finished.reshape(incoming.shape), ("sp", "tp"), split_axis=0, concat_axis=0, tiled=True
    )
    picked = returned.reshape(experts_all * capacity, model_width)[target]
    routed = jnp.sum(
        picked.reshape(rows_here, top_count, model_width).astype(jnp.float32)
        * route_weights[:, :, None],
        axis=1,
    )
    return (stream.astype(jnp.float32) + shared + routed).astype(jnp.bfloat16)


def solution(mesh):
    placed = (
        P(("grp", "sp"), None),
        P(("grp", "sp"), None),
        P(("grp", "sp"), "tp"),
        P(("grp", "sp"), "tp"),
        P(None, "tp"),
        P(None, "tp"),
        P(None, "tp"),
        P(None, "tp"),
        P(),
        P("tp", None),
        P("tp", None),
        P(("grp", "sp", "tp"), None),
        P(),
        P(None, "tp"),
        P(None, "tp"),
        P("tp", None),
        P(("sp", "tp"), None, None),
        P(("sp", "tp"), None, None),
        P(("sp", "tp"), None, None),
        P(("grp", "sp", "tp"), None),
        P(("grp", "sp", "tp"), None),
    )
    return jax.shard_map(
        body, mesh=mesh, in_specs=placed, out_specs=P(("grp", "sp", "tp"), None), check_vma=False
    )
```

profile of v0, /device:TPU:33, one launch (start us, length us, event | category | flops | bytes accessed | tf_op | source)
XLA Modules:
  0.0 667.8 jit_solution(9544668494291410742)
XLA Ops:
  11.7 112.4 %all-gather.3.cloned.1.call-done = bf16[8192,576]{0,1:T(8,128)(2,1)} async-done(((bf16[256,576]{0,1:T(8,128)(2,1)}), bf16[8192,576]{0,1:T(8,128)(2,1)}) %all-gather.3.cloned.1.call-update) | async-done | bytes 9437200 | tf_op jit(solution)/shard_map/all_gather | solution.py:17
  124.0 7.7 %slice.52 = bf16[8192,512]{0,1:T(8,128)(2,1)} slice(bf16[8192,576]{0,1:T(8,128)(2,1)} %all-gather.3.cloned.1.call-done), slice={[0:8192], [0:512]} | slice | bytes 16777216 | tf_op jit(solution)/shard_map/slice | solution.py:19
  131.7 11.9 %copy.73 = bf16[8192,512]{1,0:T(8,128)(2,1)} copy(bf16[8192,512]{0,1:T(8,128)(2,1)} %slice.52) | data formatting | bytes 16777216
  143.7 2.4 slice.54
  147.4 55.1 %while.24 = (s32[]{:T(128)}, f32[2,256]{1,0:T(2,128)S(1)}, f32[2,256]{1,0:T(2,128)}, f32[2,256,128]{2,1,0:T(8,128)S(1)}, f32[2,256]{1,0:T(2,128)S(1)}, /*index=5...) while((s32[]{:T(128)}, f32[2,256]{1,0:T(2,128)S(1)}, ...), condition=%wide.region_9.10_spmd.clone, body=%wide.region_1.9_spmd.clone.sunk | while | flops 677055232 | bytes 17331832 | solution.py:194
  150.1 10.9 %conditional.3 = ((f32[2,256]{1,0:T(2,128)S(1)}, f32[2,256]{1,0:T(2,128)}, f32[2,256,128]{2,1,0:T(8,128)S(1)}, f32[2,256]{1,0:T(2,128)S(1)}, f32[2,256]{1,0:T(2,128)S(1)}, /*index=5*/f32[2,256,64]{1,2,0:T(8,128)S(1)})) conditional(s32[]{:T(128)} %convert_element_type.225, (f32[2,256]{1,0:T(2,128)S(1)}, f32[2,256]{1,0:T(2,128)}, ...), branch_computations={%region_3.0_spmd, %region_4.8_spmd} | conditional | flops 677054720 | bytes 17326224 | solution.py:192
  205.3 2.1 fusion.36
  207.4 4.7 all-to-all-start
  212.9 25.4 %all-to-all-done = bf16[4,64,4096]{2,1,0:T(8,128)(2,1)} async-done(((bf16[4,64,4096]{2,1,0:T(8,128)(2,1)}), bf16[4,64,4096]{2,1,0:T(8,128)(2,1)}, u32[]{:S(2)}, u32[]{:S(2)}) %all-to-all-start) | async-done | bytes 2097184 | tf_op jit(solution)/shard_map/all_to_all | solution.py:31
  242.9 4.4 reshape.227
  247.3 269.1 %all_to_all.15 = bf16[128,2,4096]{2,1,0:T(2,128)(2,1)S(1)} all-to-all(bf16[128,2,4096]{2,1,0:T(2,128)(2,1)} %reshape.227), channel_id=1, replica_groups=mesh['grp'=2,'sp'=32,'tp'=4] {'sp','tp'}, dimensions={0} | all-to-all | bytes 4194304 | tf_op jit(solution)/shard_map/all_to_all | solution.py:236
  517.7 2.5 fusion.44
  520.2 7.6 %convolution_convert_fusion.5 = bf16[128,2,4096]{2,0,1:T(8,128)(2,1)} fusion(bf16[1,192,4096]{2,1,0:T(8,128)(2,1)} %param.43, bf16[1,4096,192]{1,2,0:T(8,128)(2,1)} %param.42, bf16[128,2,4096]{2,1,0:T(2,128)(2,1)} %copy-done.1, f32[128,1,2,192]{0,3,2,1:T(8,128)S(1)} %fusion.44), kind=kOutput, calls=%fused_computation.55 | convolution fusion | flops 806649856 | bytes 7536640 | tf_op jit(solution)/shard_map/sxcf,xfd->sxcd/dot_general | solution.py:244
  527.8 5.1 copy.81
  532.9 9.9 %all-to-all-start.2 = ((bf16[128,2,4096]{2,1,0:T(2,128)(2,1)}), bf16[128,2,4096]{2,1,0:T(2,128)(2,1)}, u32[]{:S(2)}, u32[]{:S(2)}) async-start(bf16[128,2,4096]{2,1,0:T(2,128)(2,1)} %copy.81), calls=%async_computation.3 | async-start | bytes 4194304 | tf_op jit(solution)/shard_map/all_to_all | solution.py:247
  543.7 45.4 %all-gather.5.cloned.1.call-done = bf16[256,4096]{1,0:T(8,128)(2,1)} async-done(((bf16[64,4096]{1,0:T(8,128)(2,1)}), bf16[256,4096]{1,0:T(8,128)(2,1)}) %all-gather.5.cloned.1.call-update) | async-done | bytes 2097168 | tf_op jit(solution)/shard_map/all_gather | solution.py:207
  589.1 2.5 fusion.105
  591.6 4.8 convolution_convert_fusion.4
  597.2 43.5 %all-to-all-done.2 = bf16[128,2,4096]{2,1,0:T(2,128)(2,1)} async-done(((bf16[128,2,4096]{2,1,0:T(2,128)(2,1)}), bf16[128,2,4096]{2,1,0:T(2,128)(2,1)}, u32[]{:S(2)}, u32[]{:S(2)}) %all-to-all-start.2) | async-done | bytes 2097184 | tf_op jit(solution)/shard_map/all_to_all | solution.py:247
  640.8 4.1 reshape.232
  644.9 5.1 gather_fusion
  649.9 3.4 reshape.233
  653.3 5.7 multiply_reduce_fusion
  658.9 2.3 fusion.79
  (151 shorter events, 60.9 us)
Async XLA Ops:
  6.5 198.7 %copy-start = (bf16[256,4096]{1,0:T(8,128)(2,1)S(1)}, bf16[256,4096]{1,0:T(8,128)(2,1)}, u32[]{:S(2)}) copy-start(bf16[256,4096]{1,0:T(8,128)(2,1)} %param.34) | copy-start | bytes 6291460
  6.6 4.0 copy-start.10
  6.6 4.1 copy-start.9
  6.6 117.5 %all-gather.3.cloned.1.call-start = ((), (), s32[]{:S(2)}) async-start(), calls=%async_computation.4 | async-start | bytes 9732096 | tf_op jit(solution)/shard_map/all_gather | solution.py:17
  143.7 3.7 copy-start.2
  143.7 3.7 copy-start.3
  143.7 3.7 copy-start.5
  143.7 3.7 copy-start.6
  156.8 1.6 copy-start.7
  158.4 1.6 copy-start.11
  160.1 0.9 copy-start.12
  207.4 4.7 copy-start.14
  207.4 30.8 %all-to-all-start = ((bf16[4,64,4096]{2,1,0:T(8,128)(2,1)}), bf16[4,64,4096]{2,1,0:T(8,128)(2,1)}, u32[]{:S(2)}, u32[]{:S(2)}) async-start(bf16[4,64,4096]{2,1,0:T(8,128)(2,1)} %bitcast.123), calls=%async_computation | async-start | bytes 4194304 | tf_op jit(solution)/shard_map/all_to_all | solution.py:31
  212.1 28.2 %copy-start.8 = (bf16[64,4096]{1,0:T(8,128)(2,1)S(1)}, bf16[64,4096]{1,0:T(8,128)(2,1)}, u32[]{:S(2)}) copy-start(bf16[64,4096]{1,0:T(8,128)(2,1)} %param.36) | copy-start | bytes 1572868
  212.9 27.7 %copy-start.13 = (f32[4096]{0:T(1024)S(1)}, f32[4096]{0:T(1024)}, u32[]{:S(2)}) copy-start(f32[4096]{0:T(1024)} %param.37) | copy-start | bytes 49156
  240.8 6.5 copy-start.4
  247.3 270.4 %copy-start.16 = (bf16[1,4096,192]{1,2,0:T(8,128)(2,1)S(1)}, bf16[1,4096,192]{1,2,0:T(8,128)(2,1)}, u32[]{:S(2)}) copy-start(bf16[1,4096,192]{1,2,0:T(8,128)(2,1)} %param.41) | copy-start | bytes 4718596
  516.4 1.3 copy-start.1
  532.9 107.8 %all-to-all-start.2 = ((bf16[128,2,4096]{2,1,0:T(2,128)(2,1)}), bf16[128,2,4096]{2,1,0:T(2,128)(2,1)}, u32[]{:S(2)}, u32[]{:S(2)}) async-start(bf16[128,2,4096]{2,1,0:T(2,128)(2,1)} %copy.81), calls=%async_computation.3 | async-start | bytes 4194304 | tf_op jit(solution)/shard_map/all_to_all | solution.py:247
  542.8 46.2 %all-gather.5.cloned.1.call-start = ((), (), s32[]{:S(2)}) async-start(), calls=%async_computation.5 | async-start | bytes 2621440 | tf_op jit(solution)/shard_map/all_gather | solution.py:207
  543.6 115.3 %reduce-scatter.2.cloned.1.call-start = ((), (), s32[]{:S(2)}) async-start(), calls=%async_computation.6 | async-start | bytes 2621440 | tf_op jit(solution)/shard_map/reduce_scatter | solution.py:212
  596.4 0.7 copy-start.15
Sparse Core Ops, SparseCore 0:
  10.7 113.3 all-gather.2
  545.5 43.5 all-gather.4
  596.6 40.5 reduce-scatter.1
where the time goes:
time: 674 us; the launch traced here: 668 us
  blocking collectives  269 us (40%)
  waiting for transfers between devices  227 us (34%)
  local copies, waits for them, and re-layouts  58.7 us (9%)
  other arithmetic  39.3 us (6%)
  matrix products  33.3 us (5%)
  starting transfers between devices  14.7 us (2%)
  between operations  13.5 us (2%)
  loops' own time  11.8 us (2%)
    all_to_all x1, blocking collectives, body(): lax.all_to_all(outgoing, ('sp', 'tp'), split_axis=0, concat_axis=0, tiled...  269 us
    all_gather x1, waiting for transfers between devices, sent_together(): whole, at, outs = (lax.all_gather(both, axis, axis=dim, tiled=True), 0, [])  112 us
    all_gather x1, waiting for transfers between devices, body(): piece = lax.all_gather(normed, 'tp', axis=0, tiled=True)  45.4 us
    all_to_all x1, waiting for transfers between devices, body(): lax.all_to_all(finished.reshape(incoming.shape), ('sp', 'tp'), split_axis...  43.5 us
    all_to_all x1, waiting for transfers between devices, summed_on_arrival(): blocks = lax.all_to_all(split_up(array, dim, peers), axis, 0, 0, tiled=True)  25.4 us
    reduce_min x16, other arithmetic, one_block(): jnp.min(key_pos) <= last_pos  23.3 us
    unnamed x35, local copies, waits for them, and re-layouts  15.4 us
  transfers between devices with their start and end apart: 5, of which 4 were waited for; matrix products, arithmetic and copies ran while one was open for 4% of the time, Pallas kernels for 0%

commit v1 on v0

--- a/solution.py
+++ b/solution.py
@@ -204,7 +204,12 @@
     )
     stream = (residual.astype(jnp.float32) + projected).astype(jnp.bfloat16)
     normed = rms_scale(stream.astype(jnp.float32), ffn_gain).astype(jnp.bfloat16)
-    piece = lax.all_gather(normed, "tp", axis=0, tiled=True)
+    ring = [normed]
+    for hop in range(3):
+        ring.append(lax.ppermute(ring[-1], "tp", [(dev, (dev + 1) % 4) for dev in range(4)]))
+    piece = jnp.roll(
+        jnp.concatenate(ring[::-1], axis=0), (lax.axis_index("tp") + 1) * ring[0].shape[0], axis=0
+    )
     gate_part = jnp.dot(piece, shared_gate, preferred_element_type=jnp.float32)
     up_part = jnp.dot(piece, shared_up, preferred_element_type=jnp.float32)
     active = (jax.nn.silu(gate_part) * up_part).astype(jnp.bfloat16)

time: 674 us -> 662 us (0.982)
  blocking collectives: 269 us -> 0 us
  starting transfers between devices: 14.7 us -> 191 us
  waiting for transfers between devices: 227 us -> 310 us
    all_to_all x1 -> x0, blocking collectives: 269 us -> none  [body(): lax.all_to_all(outgoing, ('sp', 'tp'), split_axis=0, concat_axis=0, tiled...]
    all_to_all x0 -> x1, starting transfers between devices: none -> 171 us  [body(): lax.all_to_all(outgoing, ('sp', 'tp'), split_axis=0, concat_axis=0, tiled...]
    all_to_all x0 -> x1, waiting for transfers between devices: none -> 47.5 us  [body(): lax.all_to_all(outgoing, ('sp', 'tp'), split_axis=0, concat_axis=0, tiled...]
    all_gather x1 -> x0, waiting for transfers between devices: 45.4 us -> none  [body(): piece = lax.all_gather(normed, 'tp', axis=0, tiled=True)]
    ppermute x0 -> x3, waiting for transfers between devices: none -> 42.1 us  [body(): lax.ppermute(ring[-1], 'tp', [(dev, (dev + 1) % 4) for dev in range(4)])]
    all_to_all x1, waiting for transfers between devices: 43.5 us -> 83.1 us  [body(): lax.all_to_all(finished.reshape(incoming.shape), ('sp', 'tp'), split_axis...]
    unnamed x35 -> x47, local copies, waits for them, and re-layouts: 15.4 us -> 22 us
  transfers between devices with their start and end apart: 5 -> 8, of which waited for: 4 -> 7; matrix products, arithmetic and copies ran while one was open for 4% -> 5% of each run, Pallas kernels for 0% -> 0%
where the time goes in v1:
time: 662 us; the launch traced here: 655 us
  waiting for transfers between devices  310 us (47%)
  starting transfers between devices  191 us (29%)
  local copies, waits for them, and re-layouts  59.5 us (9%)
  other arithmetic  38.7 us (6%)
  matrix products  32 us (5%)
  between operations  13.8 us (2%)
  loops' own time  9.97 us (2%)
    all_to_all x1, starting transfers between devices, body(): lax.all_to_all(outgoing, ('sp', 'tp'), split_axis=0, concat_axis=0, tiled...  171 us
    all_gather x1, waiting for transfers between devices, sent_together(): whole, at, outs = (lax.all_gather(both, axis, axis=dim, tiled=True), 0, [])  112 us
    all_to_all x1, waiting for transfers between devices, body(): lax.all_to_all(finished.reshape(incoming.shape), ('sp', 'tp'), split_axis...  83.1 us
    all_to_all x1, waiting for transfers between devices, body(): lax.all_to_all(outgoing, ('sp', 'tp'), split_axis=0, concat_axis=0, tiled...  47.5 us
    ppermute x3, waiting for transfers between devices, body(): lax.ppermute(ring[-1], 'tp', [(dev, (dev + 1) % 4) for dev in range(4)])  42.1 us
    all_to_all x1, waiting for transfers between devices, summed_on_arrival(): blocks = lax.all_to_all(split_up(array, dim, peers), axis, 0, 0, tiled=True)  25.1 us
    reduce_min x16, other arithmetic, one_block(): jnp.min(key_pos) <= last_pos  22.2 us
    unnamed x47, local copies, waits for them, and re-layouts  22 us
  transfers between devices with their start and end apart: 8, of which 7 were waited for; matrix products, arithmetic and copies ran while one was open for 5% of the time, Pallas kernels for 0%

profile of v1, /device:TPU:33, one launch (start us, length us, event | category | flops | bytes accessed | tf_op | source)
XLA Modules:
  0.0 655.4 jit_solution(14035246746597144407)
XLA Ops:
  11.7 112.4 %all-gather.2.cloned.1.call-done = bf16[8192,576]{0,1:T(8,128)(2,1)} async-done(((bf16[256,576]{0,1:T(8,128)(2,1)}), bf16[8192,576]{0,1:T(8,128)(2,1)}) %all-gather.2.cloned.1.call-update) | async-done | bytes 9437200 | tf_op jit(solution)/shard_map/all_gather | solution.py:17
  124.0 7.7 %slice.52 = bf16[8192,512]{0,1:T(8,128)(2,1)} slice(bf16[8192,576]{0,1:T(8,128)(2,1)} %all-gather.2.cloned.1.call-done), slice={[0:8192], [0:512]} | slice | bytes 16777216 | tf_op jit(solution)/shard_map/slice | solution.py:19
  131.8 11.9 %copy.73 = bf16[8192,512]{1,0:T(8,128)(2,1)} copy(bf16[8192,512]{0,1:T(8,128)(2,1)} %slice.52) | data formatting | bytes 16777216
  143.6 2.4 slice.54
  147.3 52.3 %while.24 = (s32[]{:T(128)}, f32[2,256]{1,0:T(2,128)S(1)}, f32[2,256]{1,0:T(2,128)}, f32[2,256,128]{2,1,0:T(8,128)S(1)}, f32[2,256]{1,0:T(2,128)S(1)}, /*index=5...) while((s32[]{:T(128)}, f32[2,256]{1,0:T(2,128)S(1)}, ...), condition=%wide.region_9.10_spmd.clone, body=%wide.region_1.9_spmd.clone.sunk | while | flops 677055232 | bytes 17331832 | solution.py:194
  149.9 10.9 %conditional.3 = ((f32[2,256]{1,0:T(2,128)S(1)}, f32[2,256]{1,0:T(2,128)}, f32[2,256,128]{2,1,0:T(8,128)S(1)}, f32[2,256]{1,0:T(2,128)S(1)}, f32[2,256]{1,0:T(2,128)S(1)}, /*index=5*/f32[2,256,64]{1,2,0:T(8,128)S(1)})) conditional(s32[]{:T(128)} %convert_element_type.232, (f32[2,256]{1,0:T(2,128)S(1)}, f32[2,256]{1,0:T(2,128)}, ...), branch_computations={%region_3.0_spmd, %region_4.8_spmd} | conditional | flops 677054720 | bytes 17326224 | solution.py:192
  204.6 4.1 all-to-all-start
  209.5 25.1 %all-to-all-done = bf16[4,64,4096]{2,1,0:T(8,128)(2,1)S(1)} async-done(((bf16[4,64,4096]{2,1,0:T(8,128)(2,1)}), bf16[4,64,4096]{2,1,0:T(8,128)(2,1)S(1)}, u32[]{:S(2)}, u32[]{:S(2)}) %all-to-all-start) | async-done | bytes 2097184 | tf_op jit(solution)/shard_map/all_to_all | solution.py:31
  236.2 2.7 reshape.227
  238.8 171.4 %all-to-all-start.1 = ((bf16[128,2,4096]{2,1,0:T(2,128)(2,1)}), bf16[128,2,4096]{2,1,0:T(2,128)(2,1)S(1)}, u32[]{:S(2)}, u32[]{:S(2)}) async-start(bf16[128,2,4096]{2,1,0:T(2,128)(2,1)} %reshape.227), calls=%async_computation.2 | async-start | bytes 4194304 | tf_op jit(solution)/shard_map/all_to_all | solution.py:241
  411.7 14.7 %collective-permute-done = bf16[64,4096]{1,0:T(8,128)(2,1)S(1)} collective-permute-done((bf16[64,4096]{1,0:T(8,128)(2,1)S(1)}, bf16[64,4096]{1,0:T(8,128)(2,1)S(1)}, u32[]{:S(2)}, u32[]{:S(2)}) %collective-permute-start) | collective-permute-done | bytes 524320 | tf_op jit(solution)/shard_map/ppermute | solution.py:209
  429.0 13.4 %collective-permute-done.1 = bf16[64,4096]{1,0:T(8,128)(2,1)S(1)} collective-permute-done((bf16[64,4096]{1,0:T(8,128)(2,1)S(1)}, bf16[64,4096]{1,0:T(8,128)(2,1)S(1)}, u32[]{:S(2)}, u32[]{:S(2)}) %collective-permute-start.1) | collective-permute-done | bytes 524320 | tf_op jit(solution)/shard_map/ppermute | solution.py:209
  442.4 2.4 collective-permute-start.2
  444.8 13.9 %collective-permute-done.2 = bf16[64,4096]{1,0:T(8,128)(2,1)} collective-permute-done((bf16[64,4096]{1,0:T(8,128)(2,1)S(1)}, bf16[64,4096]{1,0:T(8,128)(2,1)}, u32[]{:S(2)}, u32[]{:S(2)}) %collective-permute-start.2) | collective-permute-done | bytes 524320 | tf_op jit(solution)/shard_map/ppermute | solution.py:209
  460.6 47.5 %all-to-all-done.1 = bf16[128,2,4096]{2,1,0:T(2,128)(2,1)S(1)} async-done(((bf16[128,2,4096]{2,1,0:T(2,128)(2,1)}), bf16[128,2,4096]{2,1,0:T(2,128)(2,1)S(1)}, u32[]{:S(2)}, u32[]{:S(2)}) %all-to-all-start.1) | async-done | bytes 2097184 | tf_op jit(solution)/shard_map/all_to_all | solution.py:241
  508.1 3.9 fusion.48
  512.0 7.0 %convolution_convert_fusion.5 = bf16[128,2,4096]{2,0,1:T(8,128)(2,1)} fusion(bf16[1,192,4096]{2,1,0:T(8,128)(2,1)} %param.43, bf16[1,4096,192]{1,2,0:T(8,128)(2,1)} %param.42, bf16[128,2,4096]{2,1,0:T(2,128)(2,1)S(1)} %all-to-all-done.1, f32[128,1,2,192]{0,3,2,1:T(8,128)S(1)} %fusion.48), kind=kOutput, calls=%fused_computation.55 | convolution fusion | flops 806649856 | bytes 7536640 | tf_op jit(solution)/shard_map/sxcf,xfd->sxcd/dot_general | solution.py:249
  519.0 5.1 copy.81
  524.2 10.0 %all-to-all-start.2 = ((bf16[128,2,4096]{2,1,0:T(2,128)(2,1)}), bf16[128,2,4096]{2,1,0:T(2,128)(2,1)}, u32[]{:S(2)}, u32[]{:S(2)}) async-start(bf16[128,2,4096]{2,1,0:T(2,128)(2,1)} %copy.81), calls=%async_computation.3 | async-start | bytes 4194304 | tf_op jit(solution)/shard_map/all_to_all | solution.py:252
  543.9 4.3 convolution_convert_fusion.4
  549.0 83.1 %all-to-all-done.2 = bf16[128,2,4096]{2,1,0:T(2,128)(2,1)} async-done(((bf16[128,2,4096]{2,1,0:T(2,128)(2,1)}), bf16[128,2,4096]{2,1,0:T(2,128)(2,1)}, u32[]{:S(2)}, u32[]{:S(2)}) %all-to-all-start.2) | async-done | bytes 2097184 | tf_op jit(solution)/shard_map/all_to_all | solution.py:252
  632.1 2.7 reshape.232
  637.0 3.4 reshape.233
  640.4 5.8 multiply_reduce_fusion
  (169 shorter events, 76.9 us)
Async XLA Ops:
  6.5 195.9 %copy-start = (bf16[256,4096]{1,0:T(8,128)(2,1)S(1)}, bf16[256,4096]{1,0:T(8,128)(2,1)}, u32[]{:S(2)}) copy-start(bf16[256,4096]{1,0:T(8,128)(2,1)} %param.34) | copy-start | bytes 6291460
  6.6 4.0 copy-start.15
  6.6 4.1 copy-start.13
  6.6 117.5 %all-gather.2.cloned.1.call-start = ((), (), s32[]{:S(2)}) async-start(), calls=%async_computation.4 | async-start | bytes 9732096 | tf_op jit(solution)/shard_map/all_gather | solution.py:17
  143.6 3.6 copy-start.2
  143.6 3.6 copy-start.3
  143.6 3.7 copy-start.4
  143.6 3.7 copy-start.5
  158.2 1.6 copy-start.16
  204.6 4.1 copy-start.18
  204.6 30.0 %all-to-all-start = ((bf16[4,64,4096]{2,1,0:T(8,128)(2,1)}), bf16[4,64,4096]{2,1,0:T(8,128)(2,1)S(1)}, u32[]{:S(2)}, u32[]{:S(2)}) async-start(bf16[4,64,4096]{2,1,0:T(8,128)(2,1)} %bitcast.121), calls=%async_computation | async-start | bytes 4194304 | tf_op jit(solution)/shard_map/all_to_all | solution.py:31
  208.7 26.2 %copy-start.12 = (bf16[64,4096]{1,0:T(8,128)(2,1)S(1)}, bf16[64,4096]{1,0:T(8,128)(2,1)}, u32[]{:S(2)}) copy-start(bf16[64,4096]{1,0:T(8,128)(2,1)} %param.36) | copy-start | bytes 1572868
  209.5 25.7 %copy-start.14 = (f32[4096]{0:T(1024)S(1)}, f32[4096]{0:T(1024)}, u32[]{:S(2)}) copy-start(f32[4096]{0:T(1024)} %param.37) | copy-start | bytes 49156
  238.8 269.3 %all-to-all-start.1 = ((bf16[128,2,4096]{2,1,0:T(2,128)(2,1)}), bf16[128,2,4096]{2,1,0:T(2,128)(2,1)S(1)}, u32[]{:S(2)}, u32[]{:S(2)}) async-start(bf16[128,2,4096]{2,1,0:T(2,128)(2,1)} %reshape.227), calls=%async_computation.2 | async-start | bytes 4194304 | tf_op jit(solution)/shard_map/all_to_all | solution.py:241
  410.2 16.2 %collective-permute-start = (bf16[64,4096]{1,0:T(8,128)(2,1)S(1)}, bf16[64,4096]{1,0:T(8,128)(2,1)S(1)}, u32[]{:S(2)}, u32[]{:S(2)}) collective-permute-start(bf16[64,4096]{1,0:T(8,128)(2,1)S(1)} %fusion.80), channel_id=1, source_target_pairs={{0,1},{1,2},{2,3},{3,0},{4,5},{5,6},{6,7},{7,4},{8,9},{9,10},{10,1... | collective-permute-start | bytes 1572872 | tf_op jit(solution)/shard_map/ppermute | solution.py:209
  427.2 15.2 %collective-permute-start.1 = (bf16[64,4096]{1,0:T(8,128)(2,1)S(1)}, bf16[64,4096]{1,0:T(8,128)(2,1)S(1)}, u32[]{:S(2)}, u32[]{:S(2)}) collective-permute-start(bf16[64,4096]{1,0:T(8,128)(2,1)S(1)} %collective-permute-done), channel_id=1, source_target_pairs={{0,1},{1,2},{2,3},{3,0},{4,5},{5,6},{6,7},{7,4},{8,9},{9,10},{10,1... | collective-permute-start | bytes 1572872 | tf_op jit(solution)/shard_map/ppermute | solution.py:209
  442.4 16.2 %collective-permute-start.2 = (bf16[64,4096]{1,0:T(8,128)(2,1)S(1)}, bf16[64,4096]{1,0:T(8,128)(2,1)}, u32[]{:S(2)}, u32[]{:S(2)}) collective-permute-start(bf16[64,4096]{1,0:T(8,128)(2,1)S(1)} %collective-permute-done.1), channel_id=1, source_target_pairs={{0,1},{1,2},{2,3},{3,0},{4,5},{5,6},{6,7},{7,4},{8,9},{9,10},{10,1... | collective-permute-start | bytes 1572872 | tf_op jit(solution)/shard_map/ppermute | solution.py:209
  524.2 10.9 %copy-start.8 = (bf16[64,4096]{1,0:T(8,128)(2,1)S(1)}, bf16[64,4096]{1,0:T(8,128)(2,1)}, u32[]{:S(2)}) copy-start(bf16[64,4096]{1,0:T(8,128)(2,1)} %copy-done.7) | copy-start | bytes 1572868
  524.2 107.9 %all-to-all-start.2 = ((bf16[128,2,4096]{2,1,0:T(2,128)(2,1)}), bf16[128,2,4096]{2,1,0:T(2,128)(2,1)}, u32[]{:S(2)}, u32[]{:S(2)}) async-start(bf16[128,2,4096]{2,1,0:T(2,128)(2,1)} %copy.81), calls=%async_computation.3 | async-start | bytes 4194304 | tf_op jit(solution)/shard_map/all_to_all | solution.py:252
  534.2 112.0 %reduce-scatter.2.cloned.1.call-start = ((), (), s32[]{:S(2)}) async-start(), calls=%async_computation.5 | async-start | bytes 2621440 | tf_op jit(solution)/shard_map/reduce_scatter | solution.py:217
  536.9 4.6 copy-start.11
  540.6 3.3 copy-start.9
  540.6 3.3 copy-start.10
  640.4 8.1 %copy-start.1 = (bf16[256,4096]{1,0:T(8,128)(2,1)S(1)}, bf16[256,4096]{1,0:T(8,128)(2,1)}, u32[]{:S(2)}) copy-start(bf16[256,4096]{1,0:T(8,128)(2,1)} %param.34) | copy-start | bytes 6291460
  (4 other events, 4.0 us)
Sparse Core Ops, SparseCore 0:
  10.7 113.3 all-gather.1
  548.4 42.1 reduce-scatter.1
